TPU v7x, 32 devices: a whole 2x2x4 slice. The times are simulated.
32 devices in a mesh: ep: 8 (over z, y), tp: 4 (over x, core).
Axes of the slice: x: 2, y: 2, z: 4, core: 2. Of those that a mesh axis runs over, the one named last changes fastest.
Arguments:
- tokens: bfloat16 [256, 2048], P('ep'), may hold values from -6 to 6
- gain_mix: bfloat16 [2048], replicated, may hold values from 0.099609375 to 1.8984375
- gain_ffn: bfloat16 [2048], replicated, may hold values from 0.099609375 to 1.8984375
- w_query: bfloat16 [2048, 1024], P('ep', 'tp'), may hold values from -0.125 to 0.125
- w_key: bfloat16 [2048, 1024], P('ep', 'tp'), may hold values from -0.125 to 0.125
- w_value: bfloat16 [2048, 1024], P('ep', 'tp'), may hold values from -0.125 to 0.125
- w_outgate: bfloat16 [2048, 1024], P('ep', 'tp'), may hold values from -0.125 to 0.125
- w_ingate: bfloat16 [2048, 8], replicated, may hold values from -0.125 to 0.125
- w_forget: bfloat16 [2048, 8], replicated, may hold values from -0.125 to 0.125
- bias_in: float32 [8], replicated, may hold values from -2 to 2
- bias_forget: float32 [8], replicated, may hold values from -1 to 3
- w_proj: bfloat16 [1024, 2048], P('tp'), may hold values from -0.1875 to 0.1875
- matrix_state: float32 [256, 8, 128, 128], P('ep', 'tp'), may hold values from -0.6 to 0.6
- normal_state: float32 [256, 8, 128], P('ep', 'tp'), may hold values from -0.6 to 0.6
- stab_state: float32 [256, 8], P('ep', 'tp'), may hold values from -1 to 1
- route_ids: int32 [256, 2], P('ep'), may hold values from 0 to 3, all different within a row; in each aligned block of 32 rows (0 to 31, 32 to 63, ...) at most 32 rows name the same one
- route_weights: float32 [256, 2], P('ep'), may hold values from 0.1 to 1
- w_exp_gate: bfloat16 [8, 2048, 1536], P('ep', None, 'tp'), may hold values from -0.125 to 0.125
- w_exp_up: bfloat16 [8, 2048, 1536], P('ep', None, 'tp'), may hold values from -0.125 to 0.125
- w_exp_down: bfloat16 [8, 1536, 2048], P('ep', 'tp'), may hold values from -0.109375 to 0.109375
Outputs:
- mixed_out: bfloat16 [256, 2048], P('ep', 'tp')
- matrix_out: float32 [256, 8, 128, 128], P('ep', 'tp')
- normal_out: float32 [256, 8, 128], P('ep', 'tp')
- stab_out: float32 [256, 8], P('ep', 'tp')
Inputs may be any that keep to these rules, and one draw needn't show every extreme that they name: `route_ids`: each row names 2 different experts; among the rows of one index of ep no expert is named by more than 32 rows, and in every draw some expert is named by exactly 32 of them.
All inputs are finite; a program needn't handle non-finite values.
Results may differ from a plain program's by a relative error of at most 0.015.
Values may be sent and summed in bfloat16 or wider, within the bound.
No kernel may reach another device: no remote copies, remote signals or barrier semaphores. Data moves between devices by JAX's collectives and lax.ppermute only.
A program may use at most 64 MiB of HBM per device.

v0:
```python
import jax
import jax.numpy as jnp
from jax import lax
from jax.sharding import PartitionSpec as P

norm_epsilon = 1e-06


def rms_scale(row_block, gain):
    wide = row_block.astype(jnp.float32)
    factor = lax.rsqrt(jnp.mean(wide * wide, axis=-1, keepdims=True) + norm_epsilon)
    return (wide * factor * gain.astype(jnp.float32)).astype(jnp.bfloat16)


def memory_step(
    query,
    key_rows,
    value_rows,
    gate_rows,
    in_pre,
    forget_pre,
    matrix_state,
    normal_state,
    stab_state,
):
    log_forget = jax.nn.log_sigmoid(forget_pre)
    stab_new = jnp.maximum(log_forget + stab_state, in_pre)
    carry = jnp.exp(log_forget + stab_state - stab_new)
    inflow = jnp.exp(in_pre - stab_new)
    scaled_keys = key_rows.astype(jnp.float32) * query.shape[-1] ** (-0.5)
    value_wide = value_rows.astype(jnp.float32)
    matrix_new = (
        carry[..., None, None] * matrix_state
        + inflow[..., None, None] * scaled_keys[..., :, None] * value_wide[..., None, :]
    )
    normal_new = carry[..., None] * normal_state + inflow[..., None] * scaled_keys
    query_wide = query.astype(jnp.float32)
    numer = jnp.einsum("shd,shde->she", query_wide, matrix_new, precision=lax.Precision.HIGHEST)
    denom = jnp.maximum(jnp.abs(jnp.sum(query_wide * normal_new, axis=-1)), 1.0)
    hidden = numer / denom[..., None] * jax.nn.sigmoid(gate_rows.astype(jnp.float32))
    return (hidden, matrix_new, normal_new, stab_new)


def dispatch_table(route_ids, experts, capacity):
    flat_ids = route_ids.reshape(-1)
    expert_hot = (flat_ids[:, None] == jnp.arange(experts, dtype=jnp.int32)[None, :]).astype(
        jnp.int32
    )
    slot_rank = jnp.sum((jnp.cumsum(expert_hot, axis=0) - 1) * expert_hot, axis=1)
    slot_hot = (slot_rank[:, None] == jnp.arange(capacity, dtype=jnp.int32)[None, :]).astype(
        jnp.float32
    )
    table = expert_hot.astype(jnp.float32)[:, :, None] * slot_hot[:, None, :]
    return table.reshape(flat_ids.shape[0], experts * capacity)


def pack_rows(table, row_block, top_count, experts, capacity):
    repeated = jnp.repeat(row_block, top_count, axis=0)
    packed = jnp.einsum(
        "as,aw->sw", table.astype(jnp.bfloat16), repeated, preferred_element_type=jnp.float32
    ).astype(jnp.bfloat16)
    return packed.reshape(experts, capacity, row_block.shape[1])


def swap(value, axis, bit):
    count = lax.axis_size(axis)
    return lax.ppermute(value, axis, [(i, i ^ bit) for i in range(count)])


def bits_of(count):
    return [1 << place for place in range(count.bit_length() - 1)]


def scatter_columns(terms, axis):
    count = lax.axis_size(axis)
    index = lax.axis_index(axis)
    width = terms.shape[1] // count

    def block(peer):
        return lax.dynamic_slice_in_dim(terms, (index ^ peer) * width, width, 1)

    total = block(0)
    for peer in range(1, count):
        total = total + swap(block(peer).astype(jnp.bfloat16), axis, peer).astype(jnp.float32)
    return total


def halve_columns(terms, axis):
    count = lax.axis_size(axis)
    index = lax.axis_index(axis)
    rows, columns = terms.shape
    blocks = terms.reshape(rows, count, columns // count)
    for bit in bits_of(count):
        pairs = blocks.reshape(rows, -1, 2, blocks.shape[-1])
        own = index // bit % 2
        kept = jnp.where(own == 0, pairs[:, :, 0], pairs[:, :, 1])
        sent = jnp.where(own == 0, pairs[:, :, 1], pairs[:, :, 0]).astype(jnp.bfloat16)
        blocks = kept + swap(sent, axis, bit).astype(jnp.float32)
    return blocks.reshape(rows, columns // count)


def gather_columns(own, axis):
    count = lax.axis_size(axis)
    index = lax.axis_index(axis)
    held = own[None]
    for bit in reversed(bits_of(count)):
        other = swap(held, axis, bit)
        first = index // bit % 2 == 0
        low = jnp.where(first, held, other)
        high = jnp.where(first, other, held)
        held = jnp.stack([low, high], axis=1).reshape((-1,) + own.shape)
    return held


def body(
    tokens,
    gain_mix,
    gain_ffn,
    w_query,
    w_key,
    w_value,
    w_outgate,
    w_ingate,
    w_forget,
    bias_in,
    bias_forget,
    w_proj,
    matrix_state,
    normal_state,
    stab_state,
    route_ids,
    route_weights,
    w_exp_gate,
    w_exp_up,
    w_exp_down,
):
    ep_count = lax.axis_size("ep")
    tp_count = lax.axis_size("tp")
    ep_index = lax.axis_index("ep")
    tp_index = lax.axis_index("tp")
    seq_dev = tokens.shape[0]
    model_width = tokens.shape[1]
    heads_dev = matrix_state.shape[1]
    head_dim = matrix_state.shape[2]
    head_cols = w_query.shape[1]
    feature_rows = w_query.shape[0]
    top_count = route_ids.shape[1]
    experts = ep_count // 2
    capacity = min(seq_dev, max(2, 2 * seq_dev * top_count // experts))
    every_row = capacity == seq_dev
    col_width = model_width // tp_count
    foreign = lax.all_to_all(tokens, "ep", split_axis=1, concat_axis=0, tiled=True)
    own_gain = lax.dynamic_slice_in_dim(gain_mix, ep_index * feature_rows, feature_rows, 0)
    scaled = (foreign.astype(jnp.float32) * own_gain.astype(jnp.float32)).astype(jnp.bfloat16)
    terms = jnp.concatenate(
        [
            jnp.dot(scaled, weight, preferred_element_type=jnp.float32).astype(jnp.bfloat16)
            for weight in (w_query, w_key, w_value, w_outgate)
        ],
        axis=1,
    )
    arrived = lax.all_to_all(terms, "ep", split_axis=0, concat_axis=0, tiled=True)
    wide = tokens.astype(jnp.float32)
    factor = lax.rsqrt(jnp.mean(wide * wide, axis=-1, keepdims=True) + norm_epsilon)
    summed = factor * jnp.sum(
        arrived.astype(jnp.float32).reshape(ep_count, seq_dev, 4 * head_cols), axis=0
    )
    query, key_rows, value_rows, gate_rows = [
        summed[:, offset * head_cols : (offset + 1) * head_cols]
        .astype(jnp.bfloat16)
        .reshape(seq_dev, heads_dev, head_dim)
        for offset in range(4)
    ]
    normed = (wide * factor * gain_mix.astype(jnp.float32)).astype(jnp.bfloat16)
    head_first = tp_index * heads_dev
    in_pre = lax.dynamic_slice_in_dim(
        jnp.dot(normed, w_ingate, preferred_element_type=jnp.float32) + bias_in,
        head_first,
        heads_dev,
        1,
    )
    forget_pre = lax.dynamic_slice_in_dim(
        jnp.dot(normed, w_forget, preferred_element_type=jnp.float32) + bias_forget,
        head_first,
        heads_dev,
        1,
    )
    hidden, matrix_new, normal_new, stab_new = memory_step(
        query,
        key_rows,
        value_rows,
        gate_rows,
        in_pre,
        forget_pre,
        matrix_state,
        normal_state,
        stab_state,
    )
    cell = hidden.reshape(seq_dev, head_cols).astype(jnp.bfloat16)
    partial_out = jnp.dot(cell, w_proj, preferred_element_type=jnp.float32)
    own_tokens = lax.dynamic_slice_in_dim(tokens, tp_index * col_width, col_width, 1)
    attended = scatter_columns(partial_out, "tp")
    own_resid = (own_tokens.astype(jnp.float32) + attended).astype(jnp.bfloat16)
    if every_row:
        packed = jnp.broadcast_to(own_resid, (experts, seq_dev, col_width))
    else:
        table = dispatch_table(route_ids, experts, capacity)
        packed = pack_rows(table, own_resid, top_count, experts, capacity)
    outgoing = jnp.broadcast_to(packed[:, None], (experts, 2, capacity, col_width))
    received = lax.all_to_all(
        outgoing.reshape(ep_count * capacity, col_width),
        "ep",
        split_axis=0,
        concat_axis=0,
        tiled=True,
    )
    rows = gather_columns(received, "tp").transpose(1, 0, 2).reshape(-1, model_width)
    normed_ffn = rms_scale(rows, gain_ffn)
    gate_sum = jnp.dot(normed_ffn, w_exp_gate[0], preferred_element_type=jnp.float32)
    up_sum = jnp.dot(normed_ffn, w_exp_up[0], preferred_element_type=jnp.float32)
    inner = (jax.nn.silu(gate_sum) * up_sum).astype(jnp.bfloat16)
    expert_terms = jnp.dot(inner, w_exp_down[0], preferred_element_type=jnp.float32)
    half_share = halve_columns(expert_terms, "tp").astype(jnp.bfloat16)
    returned = lax.all_to_all(half_share, "ep", split_axis=0, concat_axis=0, tiled=True)
    halves = returned.astype(jnp.float32).reshape(experts, 2, capacity, col_width)
    weights = route_weights / jnp.sum(route_weights, axis=-1, keepdims=True)
    if every_row:
        chosen = route_ids[:, :, None] == jnp.arange(experts, dtype=jnp.int32)
        shares = jnp.sum(jnp.where(chosen, weights[:, :, None], 0.0), axis=1)
        routed = jnp.sum(halves * shares.T[:, None, :, None], axis=(0, 1))
    else:
        combine = jnp.sum(
            (table * weights.reshape(-1)[:, None]).reshape(seq_dev, top_count, experts * capacity),
            axis=1,
        )
        halves_summed = jnp.sum(halves, axis=1).reshape(experts * capacity, col_width)
        routed = jnp.dot(combine, halves_summed, precision=lax.Precision.HIGHEST)
    mixed_out = (own_resid.astype(jnp.float32) + routed).astype(jnp.bfloat16)
    return (mixed_out, matrix_new, normal_new, stab_new)


def solution(mesh):
    placed = (
        P("ep", None),
        P(),
        P(),
        P("ep", "tp"),
        P("ep", "tp"),
        P("ep", "tp"),
        P("ep", "tp"),
        P(),
        P(),
        P(),
        P(),
        P("tp", None),
        P("ep", "tp", None, None),
        P("ep", "tp", None),
        P("ep", "tp"),
        P("ep", None),
        P("ep", None),
        P("ep", None, "tp"),
        P("ep", None, "tp"),
        P("ep", "tp", None),
    )
    return jax.shard_map(
        body,
        mesh=mesh,
        in_specs=placed,
        out_specs=(P("ep", "tp"), P("ep", "tp", None, None), P("ep", "tp", None), P("ep", "tp")),
        check_vma=False,
    )
```

profile of v0, /device:TPU:0, one launch (start us, length us, event | category | flops | bytes accessed | tf_op | source)
XLA Modules:
  0.0 111.9 jit_solution(5496403255579965468)
XLA Ops:
  0.7 1.7 %copy.99 = bf16[4,8,8,256]{3,2,0,1:T(8,128)(2,1)} copy(bf16[4,8,8,256]{3,2,1,0:T(8,128)(2,1)} %bitcast.125) | data formatting | bytes 262144 | tf_op jit(solution)/shard_map/all_to_all | solution.py:152
  2.4 7.3 %all-to-all-start = ((bf16[32,8,256]{2,0,1:T(8,128)(2,1)}), bf16[32,8,256]{2,0,1:T(8,128)(2,1)S(1)}, u32[]{:S(2)}, u32[]{:S(2)}) async-start(bf16[32,8,256]{2,0,1:T(8,128)(2,1)} %bitcast.117), calls=%async_computation | async-start | bytes 262144 | tf_op jit(solution)/shard_map/all_to_all | solution.py:152
  10.4 1.0 fusion.30
  11.5 5.6 %all-to-all-done = bf16[32,8,256]{2,0,1:T(8,128)(2,1)S(1)} async-done(((bf16[32,8,256]{2,0,1:T(8,128)(2,1)}), bf16[32,8,256]{2,0,1:T(8,128)(2,1)S(1)}, u32[]{:S(2)}, u32[]{:S(2)}) %all-to-all-start) | async-done | bytes 131104 | tf_op jit(solution)/shard_map/all_to_all | solution.py:152
  17.0 1.1 %convolution_convert_fusion = bf16[256,256]{0,1:T(8,128)(2,1)S(1)} fusion(bf16[256,256]{1,0:T(8,128)(2,1)S(1)} %fusion.34, bf16[256,256]{1,0:T(8,128)(2,1)} %param.26), kind=kOutput, calls=%fused_computation.13 | convolution fusion | flops 33619968 | bytes 393216 | tf_op jit(solution)/shard_map/dot_general | solution.py:157
  18.2 1.2 %convolution_convert_fusion.1 = bf16[256,256]{0,1:T(8,128)(2,1)S(1)} fusion(bf16[256,256]{1,0:T(8,128)(2,1)S(1)} %fusion.34, bf16[256,256]{1,0:T(8,128)(2,1)} %param.25), kind=kOutput, calls=%fused_computation.14 | convolution fusion | flops 33619968 | bytes 393216 | tf_op jit(solution)/shard_map/dot_general | solution.py:157
  19.5 1.1 %convolution_convert_fusion.2 = bf16[256,256]{0,1:T(8,128)(2,1)S(1)} fusion(bf16[256,256]{1,0:T(8,128)(2,1)S(1)} %fusion.34, bf16[256,256]{1,0:T(8,128)(2,1)} %param.24), kind=kOutput, calls=%fused_computation.15 | convolution fusion | flops 33619968 | bytes 393216 | tf_op jit(solution)/shard_map/dot_general | solution.py:157
  20.9 1.0 copy.76
  21.9 3.5 %all-to-all-start.1 = ((bf16[8,32,1024]{2,1,0:T(8,128)(2,1)}), bf16[8,32,1024]{2,1,0:T(8,128)(2,1)S(1)}, u32[]{:S(2)}, u32[]{:S(2)}) async-start(bf16[8,32,1024]{2,1,0:T(8,128)(2,1)} %bitcast.2), calls=%async_computation.1 | async-start | bytes 1048576 | tf_op jit(solution)/shard_map/all_to_all | solution.py:162
  26.2 12.5 %all-to-all-done.1 = bf16[8,32,1024]{2,1,0:T(8,128)(2,1)S(1)} async-done(((bf16[8,32,1024]{2,1,0:T(8,128)(2,1)}), bf16[8,32,1024]{2,1,0:T(8,128)(2,1)S(1)}, u32[]{:S(2)}, u32[]{:S(2)}) %all-to-all-start.1) | async-done | bytes 524320 | tf_op jit(solution)/shard_map/all_to_all | solution.py:162
  39.0 0.8 multiply_reduce_fusion.1
  39.8 3.7 %multiply_add_fusion = f32[32,2,128,128]{3,2,1,0:T(8,128)S(1)} fusion(f32[32,2,128,128]{3,2,1,0:T(8,128)} %param.32, f32[32,2,128]{2,1,0:T(2,128)S(1)} %reshape.185, f32[32,2,128]{2,1,0:T(2,128)S(1)} %get-tuple-element.6, f32[32,2]{1,0:T(8,128)S(1)} %copy.77), kind=kLoop, calls=%fused_computation | loop fusion | flops 3145728 | bytes 8454400 | tf_op jit(solution)/shard_map/add | solution.py:33
  43.5 2.0 %fusion.48 = f32[32,2,1,128]{3,2,1,0:T(1,128)S(1)} fusion(bf16[32,2,128,1]{2,3,1,0:T(2,128)(2,1)S(1)} %reshape.194, f32[32,2,128,128]{3,2,1,0:T(8,128)S(1)} %multiply_add_fusion), kind=kOutput, calls=%fused_computation.88 | convolution fusion | flops 12582912 | bytes 4243456 | tf_op jit(solution)/shard_map/shd,shde->she/dot_general | solution.py:38
  46.1 1.6 %collective-permute-start.1 = (bf16[32,512]{1,0:T(8,128)(2,1)S(1)}, bf16[32,512]{1,0:T(8,128)(2,1)S(1)}, u32[]{:S(2)}, u32[]{:S(2)}) collective-permute-start(bf16[32,512]{1,0:T(8,128)(2,1)S(1)} %get-tuple-element.15), channel_id=1, source_target_pairs={{0,2},{1,3},{2,0},{3,1},{4,6},{5,7},{6,4},{7,5},{8,10},{9,11},{10,... | collective-permute-start | bytes 98312 | tf_op jit(solution)/shard_map/ppermute | solution.py:67
  47.9 2.1 %collective-permute-done.1 = bf16[32,512]{1,0:T(8,128)(2,1)S(1)} collective-permute-done((bf16[32,512]{1,0:T(8,128)(2,1)S(1)}, bf16[32,512]{1,0:T(8,128)(2,1)S(1)}, u32[]{:S(2)}, u32[]{:S(2)}) %collective-permute-start.1) | collective-permute-done | bytes 32800 | tf_op jit(solution)/shard_map/ppermute | solution.py:67
  50.0 0.9 collective-permute-done.2
  51.0 12.7 %all_to_all.37 = bf16[8,32,512]{2,1,0:T(8,128)(2,1)S(1)} all-to-all(bf16[8,32,512]{2,1,0:T(8,128)(2,1)S(1)} %all_to_all.30), channel_id=1, replica_groups=mesh['ep'=8,'tp'=4] {'ep'}, dimensions={0} | all-to-all | bytes 524288 | tf_op jit(solution)/shard_map/all_to_all | solution.py:210
  63.7 0.9 collective-permute-start.3
  64.6 5.7 %collective-permute-done.3 = bf16[1,256,512]{2,1,0:T(8,128)(2,1)S(1)} collective-permute-done((bf16[1,256,512]{2,1,0:T(8,128)(2,1)S(1)}, bf16[1,256,512]{2,1,0:T(8,128)(2,1)S(1)}, u32[]{:S(2)}, u32[]{:S(2)}) %collective-permute-start.3) | collective-permute-done | bytes 262176 | tf_op jit(solution)/shard_map/ppermute | solution.py:67
  70.5 2.6 %copy.90 = bf16[2048,384]{1,0:T(8,128)(2,1)} copy(bf16[2048,384]{0,1:T(8,128)(2,1)} %bitcast.121) | data formatting | bytes 3145728 | tf_op jit(solution)/shard_map/dot_general | solution.py:222
  73.6 1.3 %fusion.16 = bf16[256,4,512]{2,0,1:T(8,128)(2,1)} fusion(bf16[2,2,256,512]{3,2,1,0:T(8,128)(2,1)S(1)} %pad_maximum_fusion, f32[4,512]{1,0:T(4,128)S(1)} %reshape.189, f32[256]{0:T(256)S(1)} %add_rsqrt_fusion), kind=kLoop, calls=%fused_computation.19 | loop fusion | flops 2097152 | bytes 2106368 | tf_op jit(solution)/shard_map/convert_element_type | solution.py:12
  74.9 1.5 %copy.81 = bf16[256,4,512]{0,2,1:T(8,128)(2,1)S(1)} copy(bf16[256,4,512]{2,0,1:T(8,128)(2,1)} %fusion.16) | data formatting | bytes 2097152 | tf_op jit(solution)/shard_map/convert_element_type | solution.py:12
  76.4 2.1 %fusion.5 = f32[256,384]{1,0:T(8,128)S(1)} fusion(bf16[256,2048]{0,1:T(8,128)(2,1)S(1)} %bitcast.119, bf16[1,2048,384]{2,1,0:T(8,128)(2,1)} %param.37), kind=kOutput, calls=%fused_computation.8 | convolution fusion | flops 402653184 | bytes 3014656 | tf_op jit(solution)/shard_map/dot_general | solution.py:219
  78.6 4.1 %fusion.21 = f32[256,2,2,512]{3,0,2,1:T(8,128)} fusion(bf16[2,2,512,384]{3,2,1,0:T(8,128)(2,1)} %bitcast.122, bf16[256,2048]{0,1:T(8,128)(2,1)S(1)} %bitcast.120, bf16[1,2048,384]{2,1,0:T(8,128)(2,1)S(1)} %copy-done, f32[256,384]{1,0:T(8,128)S(1)} %fusion.5), kind=kOutput, calls=%fused_computation.27 | convolution fusion | flops 805896192 | bytes 6684672 | tf_op jit(solution)/shard_map/dot_general | solution.py:222
  82.7 1.6 %fusion.23 = bf16[256,2,512]{2,0,1:T(8,128)(2,1)S(1)} fusion(f32[256,2,2,512]{3,0,2,1:T(8,128)} %fusion.21, pred[]{:T(512)S(6)} %eq.29), kind=kLoop, calls=%fused_computation.28 | loop fusion | flops 262144 | bytes 1572865 | tf_op jit(solution)/shard_map/convert_element_type | solution.py:97
  84.9 1.5 %collective-permute-done.5 = bf16[256,2,512]{2,0,1:T(8,128)(2,1)S(1)} collective-permute-done((bf16[256,2,512]{2,0,1:T(8,128)(2,1)S(1)}, bf16[256,2,512]{2,0,1:T(8,128)(2,1)S(1)}, u32[]{:S(2)}, u32[]{:S(2)}) %collective-permute-start.5) | collective-permute-done | bytes 524320 | tf_op jit(solution)/shard_map/ppermute | solution.py:67
  86.4 1.8 %fusion.19 = f32[256,1,2,512]{3,0,2,1:T(8,128)S(1)} fusion(bf16[256,2,512]{2,0,1:T(8,128)(2,1)S(1)} %collective-permute-done.5, f32[256,2,2,512]{3,0,2,1:T(8,128)} %fusion.21, pred[]{:T(512)S(6)} %eq.29), kind=kLoop, calls=%fused_computation.24 | loop fusion | flops 786432 | bytes 3670017 | tf_op jit(solution)/shard_map/reshape | solution.py:94
  88.3 1.0 collective-permute-start.6
  89.3 7.7 %collective-permute-done.6 = bf16[256,1,512]{2,0,1:T(8,128)(2,1)S(1)} collective-permute-done((bf16[256,1,512]{2,0,1:T(8,128)(2,1)S(1)}, bf16[256,1,512]{2,0,1:T(8,128)(2,1)S(1)}, u32[]{:S(2)}, u32[]{:S(2)}) %collective-permute-start.6) | collective-permute-done | bytes 262176 | tf_op jit(solution)/shard_map/ppermute | solution.py:67
  97.0 0.8 fusion.24
  97.8 4.7 %all-to-all-start.3 = ((bf16[8,32,512]{2,1,0:T(8,128)(2,1)}), bf16[8,32,512]{2,1,0:T(8,128)(2,1)S(1)}, u32[]{:S(2)}, u32[]{:S(2)}) async-start(bf16[8,32,512]{2,1,0:T(8,128)(2,1)} %bitcast.31), calls=%async_computation.3 | async-start | bytes 524288 | tf_op jit(solution)/shard_map/all_to_all | solution.py:224
  102.6 8.5 %all-to-all-done.3 = bf16[8,32,512]{2,1,0:T(8,128)(2,1)S(1)} async-done(((bf16[8,32,512]{2,1,0:T(8,128)(2,1)}), bf16[8,32,512]{2,1,0:T(8,128)(2,1)S(1)}, u32[]{:S(2)}, u32[]{:S(2)}) %all-to-all-start.3) | async-done | bytes 262176 | tf_op jit(solution)/shard_map/all_to_all | solution.py:224
  (79 shorter events, 4.9 us)
Async XLA Ops:
  0.6 77.9 %copy-start = (bf16[1,2048,384]{2,1,0:T(8,128)(2,1)S(1)}, bf16[1,2048,384]{2,1,0:T(8,128)(2,1)}, u32[]{:S(2)}) copy-start(bf16[1,2048,384]{2,1,0:T(8,128)(2,1)} %param.38) | copy-start | bytes 4718596
  0.6 20.0 %copy-start.4 = (bf16[256,256]{1,0:T(8,128)(2,1)S(1)}, bf16[256,256]{1,0:T(8,128)(2,1)}, u32[]{:S(2)}) copy-start(bf16[256,256]{1,0:T(8,128)(2,1)} %param.23) | copy-start | bytes 393220
  2.4 14.7 %all-to-all-start = ((bf16[32,8,256]{2,0,1:T(8,128)(2,1)}), bf16[32,8,256]{2,0,1:T(8,128)(2,1)S(1)}, u32[]{:S(2)}, u32[]{:S(2)}) async-start(bf16[32,8,256]{2,0,1:T(8,128)(2,1)} %bitcast.117), calls=%async_computation | async-start | bytes 262144 | tf_op jit(solution)/shard_map/all_to_all | solution.py:152
  18.2 7.3 %copy-start.6 = (bf16[2048]{0:T(1024)(128)(2,1)S(1)}, bf16[2048]{0:T(1024)(128)(2,1)}, u32[]{:S(2)}) copy-start(bf16[2048]{0:T(1024)(128)(2,1)} %param.21) | copy-start | bytes 12292
  18.2 7.3 %copy-start.3 = (bf16[32,2048]{1,0:T(8,128)(2,1)S(1)}, bf16[32,2048]{1,0:T(8,128)(2,1)}, u32[]{:S(2)}) copy-start(bf16[32,2048]{1,0:T(8,128)(2,1)} %param.20) | copy-start | bytes 393220
  18.2 7.3 %copy-start.12 = (bf16[2048,8]{0,1:T(8,128)(2,1)S(1)}, bf16[2048,8]{0,1:T(8,128)(2,1)}, u32[]{:S(2)}) copy-start(bf16[2048,8]{0,1:T(8,128)(2,1)} %param.27) | copy-start | bytes 98308
  18.2 7.3 %copy-start.14 = (f32[8]{0:T(128)S(1)}, f32[8]{0:T(128)}, u32[]{:S(2)}) copy-start(f32[8]{0:T(128)} %param.29) | copy-start | bytes 100
  19.4 6.3 %copy-start.13 = (bf16[2048,8]{0,1:T(8,128)(2,1)S(1)}, bf16[2048,8]{0,1:T(8,128)(2,1)}, u32[]{:S(2)}) copy-start(bf16[2048,8]{0,1:T(8,128)(2,1)} %param.28) | copy-start | bytes 98308
  19.5 6.3 %copy-start.15 = (f32[8]{0:T(128)S(1)}, f32[8]{0:T(128)}, u32[]{:S(2)}) copy-start(f32[8]{0:T(128)} %param.30) | copy-start | bytes 100
  20.6 5.3 %copy-start.10 = (f32[32,2]{0,1:T(2,128)S(1)}, f32[32,2]{0,1:T(2,128)}, u32[]{:S(2)}) copy-start(f32[32,2]{0,1:T(2,128)} %param.34) | copy-start | bytes 772
  20.9 18.1 %copy-start.5 = (f32[32,2,128]{2,1,0:T(2,128)S(1)}, f32[32,2,128]{2,1,0:T(2,128)}, u32[]{:S(2)}) copy-start(f32[32,2,128]{2,1,0:T(2,128)} %param.33) | copy-start | bytes 98308
  21.9 16.8 %all-to-all-start.1 = ((bf16[8,32,1024]{2,1,0:T(8,128)(2,1)}), bf16[8,32,1024]{2,1,0:T(8,128)(2,1)S(1)}, u32[]{:S(2)}, u32[]{:S(2)}) async-start(bf16[8,32,1024]{2,1,0:T(8,128)(2,1)} %bitcast.2), calls=%async_computation.1 | async-start | bytes 1048576 | tf_op jit(solution)/shard_map/all_to_all | solution.py:162
  26.0 17.5 %copy-start.9 = (f32[32,2]{0,1:T(2,128)}, f32[32,2]{0,1:T(2,128)S(1)}, u32[]{:S(2)}) copy-start(f32[32,2]{0,1:T(2,128)S(1)} %get-tuple-element.8) | copy-start | bytes 772
  43.5 2.0 %copy-start.1 = (f32[32,2,128,128]{3,2,1,0:T(8,128)}, f32[32,2,128,128]{3,2,1,0:T(8,128)S(1)}, u32[]{:S(2)}) copy-start(f32[32,2,128,128]{3,2,1,0:T(8,128)S(1)} %multiply_add_fusion) | copy-start | bytes 12582916
  43.5 2.2 %copy-start.2 = (bf16[256,2048]{1,0:T(8,128)(2,1)S(1)}, bf16[256,2048]{1,0:T(8,128)(2,1)}, u32[]{:S(2)}) copy-start(bf16[256,2048]{1,0:T(8,128)(2,1)} %param.31) | copy-start | bytes 3145732
  45.7 24.8 %copy-start.7 = (bf16[2048]{0:T(1024)(128)(2,1)S(1)}, bf16[2048]{0:T(1024)(128)(2,1)}, u32[]{:S(2)}) copy-start(bf16[2048]{0:T(1024)(128)(2,1)} %param.22) | copy-start | bytes 12292
  46.0 1.9 %collective-permute-start = (bf16[32,512]{1,0:T(8,128)(2,1)S(1)}, bf16[32,512]{1,0:T(8,128)(2,1)S(1)}, u32[]{:S(2)}, u32[]{:S(2)}) collective-permute-start(bf16[32,512]{1,0:T(8,128)(2,1)S(1)} %get-tuple-element.13), channel_id=1, source_target_pairs={{0,1},{1,0},{2,3},{3,2},{4,5},{5,4},{6,7},{7,6},{8,9},{9,8},{10,11... | collective-permute-start | bytes 98312 | tf_op jit(solution)/shard_map/ppermute | solution.py:67
  46.1 4.0 %collective-permute-start.1 = (bf16[32,512]{1,0:T(8,128)(2,1)S(1)}, bf16[32,512]{1,0:T(8,128)(2,1)S(1)}, u32[]{:S(2)}, u32[]{:S(2)}) collective-permute-start(bf16[32,512]{1,0:T(8,128)(2,1)S(1)} %get-tuple-element.15), channel_id=1, source_target_pairs={{0,2},{1,3},{2,0},{3,1},{4,6},{5,7},{6,4},{7,5},{8,10},{9,11},{10,... | collective-permute-start | bytes 98312 | tf_op jit(solution)/shard_map/ppermute | solution.py:67
  47.6 3.4 %collective-permute-start.2 = (bf16[32,512]{1,0:T(8,128)(2,1)S(1)}, bf16[32,512]{1,0:T(8,128)(2,1)S(1)}, u32[]{:S(2)}, u32[]{:S(2)}) collective-permute-start(bf16[32,512]{1,0:T(8,128)(2,1)S(1)} %get-tuple-element.14), channel_id=1, source_target_pairs={{0,3},{1,2},{2,1},{3,0},{4,7},{5,6},{6,5},{7,4},{8,11},{9,10},{10,... | collective-permute-start | bytes 98312 | tf_op jit(solution)/shard_map/ppermute | solution.py:67
  63.7 6.6 %collective-permute-start.3 = (bf16[1,256,512]{2,1,0:T(8,128)(2,1)S(1)}, bf16[1,256,512]{2,1,0:T(8,128)(2,1)S(1)}, u32[]{:S(2)}, u32[]{:S(2)}) collective-permute-start(bf16[1,256,512]{2,1,0:T(8,128)(2,1)S(1)} %bitcast.123), channel_id=1, source_target_pairs={{0,2},{1,3},{2,0},{3,1},{4,6},{5,7},{6,4},{7,5},{8,10},{9,11},{10,... | collective-permute-start | bytes 786440 | tf_op jit(solution)/shard_map/ppermute | solution.py:67
  70.4 2.7 %collective-permute-start.4 = (bf16[2,256,512]{2,1,0:T(8,128)(2,1)S(1)}, bf16[2,256,512]{2,1,0:T(8,128)(2,1)S(1)}, u32[]{:S(2)}, u32[]{:S(2)}) collective-permute-start(bf16[2,256,512]{2,1,0:T(8,128)(2,1)S(1)} %maximum_bitcast_fusion), channel_id=1, source_target_pairs={{0,1},{1,0},{2,3},{3,2},{4,5},{5,4},{6,7},{7,6},{8,9},{9,8},{10,11... | collective-permute-start | bytes 1572872 | tf_op jit(solution)/shard_map/ppermute | solution.py:67
  84.3 2.1 %collective-permute-start.5 = (bf16[256,2,512]{2,0,1:T(8,128)(2,1)S(1)}, bf16[256,2,512]{2,0,1:T(8,128)(2,1)S(1)}, u32[]{:S(2)}, u32[]{:S(2)}) collective-permute-start(bf16[256,2,512]{2,0,1:T(8,128)(2,1)S(1)} %fusion.23), channel_id=1, source_target_pairs={{0,1},{1,0},{2,3},{3,2},{4,5},{5,4},{6,7},{7,6},{8,9},{9,8},{10,11... | collective-permute-start | bytes 1572872 | tf_op jit(solution)/shard_map/ppermute | solution.py:67
  88.3 14.3 %copy-start.8 = (f32[32,2]{0,1:T(2,128)S(1)}, f32[32,2]{0,1:T(2,128)}, u32[]{:S(2)}) copy-start(f32[32,2]{0,1:T(2,128)} %param.36) | copy-start | bytes 772
  88.3 14.3 %copy-start.11 = (s32[32,2]{0,1:T(2,128)S(1)}, s32[32,2]{0,1:T(2,128)}, u32[]{:S(2)}) copy-start(s32[32,2]{0,1:T(2,128)} %param.35) | copy-start | bytes 772
  88.3 8.7 %collective-permute-start.6 = (bf16[256,1,512]{2,0,1:T(8,128)(2,1)S(1)}, bf16[256,1,512]{2,0,1:T(8,128)(2,1)S(1)}, u32[]{:S(2)}, u32[]{:S(2)}) collective-permute-start(bf16[256,1,512]{2,0,1:T(8,128)(2,1)S(1)} %fusion.33), channel_id=1, source_target_pairs={{0,2},{1,3},{2,0},{3,1},{4,6},{5,7},{6,4},{7,5},{8,10},{9,11},{10,... | collective-permute-start | bytes 786440 | tf_op jit(solution)/shard_map/ppermute | solution.py:67
  97.8 13.3 %all-to-all-start.3 = ((bf16[8,32,512]{2,1,0:T(8,128)(2,1)}), bf16[8,32,512]{2,1,0:T(8,128)(2,1)S(1)}, u32[]{:S(2)}, u32[]{:S(2)}) async-start(bf16[8,32,512]{2,1,0:T(8,128)(2,1)} %bitcast.31), calls=%async_computation.3 | async-start | bytes 524288 | tf_op jit(solution)/shard_map/all_to_all | solution.py:224
where the time goes:
time: 113 us; the launch traced here: 112 us
  waiting for transfers between devices  44.6 us (39%)
  starting transfers between devices  19.9 us (18%)
  other arithmetic  13.7 us (12%)
  matrix products  12.7 us (11%)
  blocking collectives  12.7 us (11%)
  local copies, waits for them, and re-layouts  7.19 us (6%)
    ppermute x7, waiting for transfers between devices, swap(): return lax.ppermute(value, axis, [(i, i ^ bit) for i in range(count)])  18 us
    all_to_all x1, blocking collectives, body(): lax.all_to_all(outgoing.reshape(ep_count * capacity, col_width), 'ep', sp...  12.7 us
    all_to_all x1, waiting for transfers between devices, body(): lax.all_to_all(terms, 'ep', split_axis=0, concat_axis=0, tiled=True)  12.5 us
    all_to_all x1, waiting for transfers between devices, body(): lax.all_to_all(half_share, 'ep', split_axis=0, concat_axis=0, tiled=True)  8.54 us
    all_to_all x1, starting transfers between devices, body(): lax.all_to_all(tokens, 'ep', split_axis=1, concat_axis=0, tiled=True)  7.31 us
    all_to_all x1, waiting for transfers between devices, body(): lax.all_to_all(tokens, 'ep', split_axis=1, concat_axis=0, tiled=True)  5.55 us
    all_to_all x1, starting transfers between devices, body(): lax.all_to_all(half_share, 'ep', split_axis=0, concat_axis=0, tiled=True)  4.7 us
    ppermute x7, starting transfers between devices, swap(): return lax.ppermute(value, axis, [(i, i ^ bit) for i in range(count)])  4.37 us
  transfers between devices with their start and end apart: 10, of which 8 were waited for; matrix products, arithmetic and copies ran while one was open for 5% of the time, Pallas kernels for 0%

commit v1 on v0

--- a/solution.py
+++ b/solution.py
@@ -149,7 +149,10 @@
     capacity = min(seq_dev, max(2, 2 * seq_dev * top_count // experts))
     every_row = capacity == seq_dev
     col_width = model_width // tp_count
-    foreign = lax.all_to_all(tokens, "ep", split_axis=1, concat_axis=0, tiled=True)
+    foreign = jnp.concatenate(
+        lax.all_to_all(jnp.stack(jnp.split(tokens, lax.axis_size("ep"), axis=1)), "ep", 0, 0),
+        axis=0,
+    )
     own_gain = lax.dynamic_slice_in_dim(gain_mix, ep_index * feature_rows, feature_rows, 0)
     scaled = (foreign.astype(jnp.float32) * own_gain.astype(jnp.float32)).astype(jnp.bfloat16)
     terms = jnp.concatenate(

time: 113 us -> 122 us (1.080)
  local copies, waits for them, and re-layouts: 7.19 us -> 16.2 us
    unnamed x32 -> x39, local copies, waits for them, and re-layouts: 0.1 us -> 9.52 us
    all_to_all x1 -> x0, local copies, waits for them, and re-layouts: 1.71 us -> none  [body(): lax.all_to_all(tokens, 'ep', split_axis=1, concat_axis=0, tiled=True)]
    another operation x0 -> x1, local copies, waits for them, and re-layouts: none -> 1.32 us  [body(): jnp.stack(jnp.split(tokens, lax.axis_size('ep'), axis=1))]
  transfers between devices with their start and end apart: 10 -> 10, of which waited for: 8 -> 8; matrix products, arithmetic and copies ran while one was open for 5% -> 4% of each run, Pallas kernels for 0% -> 0%
where the time goes in v1:
time: 122 us; the launch traced here: 121 us
  waiting for transfers between devices  44.6 us (37%)
  starting transfers between devices  19.9 us (16%)
  local copies, waits for them, and re-layouts  16.2 us (13%)
  other arithmetic  13.7 us (11%)
  matrix products  12.7 us (10%)
  blocking collectives  12.7 us (10%)
    ppermute x7, waiting for transfers between devices, swap(): return lax.ppermute(value, axis, [(i, i ^ bit) for i in range(count)])  18 us
    all_to_all x1, blocking collectives, body(): lax.all_to_all(outgoing.reshape(ep_count * capacity, col_width), 'ep', sp...  12.7 us
    all_to_all x1, waiting for transfers between devices, body(): lax.all_to_all(terms, 'ep', split_axis=0, concat_axis=0, tiled=True)  12.5 us
    unnamed x39, local copies, waits for them, and re-layouts  9.52 us
    all_to_all x1, waiting for transfers between devices, body(): lax.all_to_all(half_share, 'ep', split_axis=0, concat_axis=0, tiled=True)  8.54 us
    all_to_all x1, starting transfers between devices, body(): lax.all_to_all(jnp.stack(jnp.split(tokens, lax.axis_size('ep'), axis=1)),...  7.31 us
    all_to_all x1, waiting for transfers between devices, body(): lax.all_to_all(jnp.stack(jnp.split(tokens, lax.axis_size('ep'), axis=1)),...  5.55 us
    all_to_all x1, starting transfers between devices, body(): lax.all_to_all(half_share, 'ep', split_axis=0, concat_axis=0, tiled=True)  4.7 us
  transfers between devices with their start and end apart: 10, of which 8 were waited for; matrix products, arithmetic and copies ran while one was open for 4% of the time, Pallas kernels for 0%

profile of v1, /device:TPU:0, one launch (start us, length us, event | category | flops | bytes accessed | tf_op | source)
XLA Modules:
  0.0 120.9 jit_solution(13788117370893579399)
XLA Ops:
  0.7 1.5 %constant_dynamic-update-slice_fusion.7 = bf16[8,32,256]{2,1,0:T(8,128)(2,1)} fusion(bf16[32,2048]{1,0:T(8,128)(2,1)} %param.20), kind=kLoop, calls=%fused_computation.71 | loop fusion | bytes 32768
  2.1 1.3 %constant_dynamic-update-slice_fusion.6 = bf16[8,32,256]{2,1,0:T(8,128)(2,1)} fusion(bf16[8,32,256]{2,1,0:T(8,128)(2,1)} %constant_dynamic-update-slice_fusion.7, bf16[32,2048]{1,0:T(8,128)(2,1)} %param.20), kind=kLoop, calls=%fused_computation.70 | loop fusion | bytes 32768
  3.5 1.3 %constant_dynamic-update-slice_fusion.5 = bf16[8,32,256]{2,1,0:T(8,128)(2,1)} fusion(bf16[8,32,256]{2,1,0:T(8,128)(2,1)} %constant_dynamic-update-slice_fusion.6, bf16[32,2048]{1,0:T(8,128)(2,1)} %param.20), kind=kLoop, calls=%fused_computation.69 | loop fusion | bytes 32768
  4.8 1.3 %constant_dynamic-update-slice_fusion.4 = bf16[8,32,256]{2,1,0:T(8,128)(2,1)} fusion(bf16[8,32,256]{2,1,0:T(8,128)(2,1)} %constant_dynamic-update-slice_fusion.5, bf16[32,2048]{1,0:T(8,128)(2,1)} %param.20), kind=kLoop, calls=%fused_computation.68 | loop fusion | bytes 32768
  6.1 1.3 %constant_dynamic-update-slice_fusion.3 = bf16[8,32,256]{2,1,0:T(8,128)(2,1)} fusion(bf16[8,32,256]{2,1,0:T(8,128)(2,1)} %constant_dynamic-update-slice_fusion.4, bf16[32,2048]{1,0:T(8,128)(2,1)} %param.20), kind=kLoop, calls=%fused_computation.67 | loop fusion | bytes 32768
  7.4 1.3 %constant_dynamic-update-slice_fusion.2 = bf16[8,32,256]{2,1,0:T(8,128)(2,1)} fusion(bf16[8,32,256]{2,1,0:T(8,128)(2,1)} %constant_dynamic-update-slice_fusion.3, bf16[32,2048]{1,0:T(8,128)(2,1)} %param.20), kind=kLoop, calls=%fused_computation.66 | loop fusion | bytes 32768
  8.8 1.3 %constant_dynamic-update-slice_fusion.1 = bf16[8,32,256]{2,1,0:T(8,128)(2,1)} fusion(bf16[8,32,256]{2,1,0:T(8,128)(2,1)} %constant_dynamic-update-slice_fusion.2, bf16[32,2048]{1,0:T(8,128)(2,1)} %param.20), kind=kLoop, calls=%fused_computation.65 | loop fusion | bytes 32768
  10.1 1.3 %constant_dynamic-update-slice_fusion = bf16[8,32,256]{2,1,0:T(8,128)(2,1)} fusion(bf16[8,32,256]{2,1,0:T(8,128)(2,1)} %constant_dynamic-update-slice_fusion.1, bf16[32,2048]{1,0:T(8,128)(2,1)} %param.20), kind=kLoop, calls=%fused_computation.64 | loop fusion | bytes 32768 | tf_op jit(solution)/shard_map/stack | solution.py:153
  11.4 7.3 %all-to-all-start = ((bf16[8,32,256]{2,1,0:T(8,128)(2,1)}), bf16[8,32,256]{2,1,0:T(8,128)(2,1)S(1)}, u32[]{:S(2)}, u32[]{:S(2)}) async-start(bf16[8,32,256]{2,1,0:T(8,128)(2,1)} %constant_dynamic-update-slice_fusion), calls=%async_computation | async-start | bytes 262144 | tf_op jit(solution)/shard_map/all_to_all | solution.py:153
  20.5 5.6 %all-to-all-done = bf16[8,32,256]{2,1,0:T(8,128)(2,1)S(1)} async-done(((bf16[8,32,256]{2,1,0:T(8,128)(2,1)}), bf16[8,32,256]{2,1,0:T(8,128)(2,1)S(1)}, u32[]{:S(2)}, u32[]{:S(2)}) %all-to-all-start) | async-done | bytes 131104 | tf_op jit(solution)/shard_map/all_to_all | solution.py:153
  26.1 1.1 convolution_convert_fusion
  27.3 1.2 convolution_convert_fusion.1
  28.5 1.1 convolution_convert_fusion.2
  31.0 3.5 %all-to-all-start.1 = ((bf16[8,32,1024]{2,1,0:T(8,128)(2,1)}), bf16[8,32,1024]{2,1,0:T(8,128)(2,1)S(1)}, u32[]{:S(2)}, u32[]{:S(2)}) async-start(bf16[8,32,1024]{2,1,0:T(8,128)(2,1)} %bitcast.9), calls=%async_computation.1 | async-start | bytes 1048576 | tf_op jit(solution)/shard_map/all_to_all | solution.py:165
  35.3 12.5 %all-to-all-done.1 = bf16[8,32,1024]{2,1,0:T(8,128)(2,1)S(1)} async-done(((bf16[8,32,1024]{2,1,0:T(8,128)(2,1)}), bf16[8,32,1024]{2,1,0:T(8,128)(2,1)S(1)}, u32[]{:S(2)}, u32[]{:S(2)}) %all-to-all-start.1) | async-done | bytes 524320 | tf_op jit(solution)/shard_map/all_to_all | solution.py:165
  48.8 3.7 %multiply_add_fusion = f32[32,2,128,128]{3,2,1,0:T(8,128)S(1)} fusion(f32[32,2,128,128]{3,2,1,0:T(8,128)} %param.32, f32[32,2,128]{2,1,0:T(2,128)S(1)} %reshape.183, f32[32,2,128]{2,1,0:T(2,128)S(1)} %get-tuple-element.6, f32[32,2]{1,0:T(8,128)S(1)} %copy.48), kind=kLoop, calls=%fused_computation | loop fusion | flops 3145728 | bytes 8454400 | tf_op jit(solution)/shard_map/add | solution.py:33
  52.6 2.0 %fusion.48 = f32[32,2,1,128]{3,2,1,0:T(1,128)S(1)} fusion(bf16[32,2,128,1]{2,3,1,0:T(2,128)(2,1)S(1)} %reshape.192, f32[32,2,128,128]{3,2,1,0:T(8,128)S(1)} %multiply_add_fusion), kind=kOutput, calls=%fused_computation.95 | convolution fusion | flops 12582912 | bytes 4243456 | tf_op jit(solution)/shard_map/shd,shde->she/dot_general | solution.py:38
  55.1 1.6 %collective-permute-start.1 = (bf16[32,512]{1,0:T(8,128)(2,1)S(1)}, bf16[32,512]{1,0:T(8,128)(2,1)S(1)}, u32[]{:S(2)}, u32[]{:S(2)}) collective-permute-start(bf16[32,512]{1,0:T(8,128)(2,1)S(1)} %get-tuple-element.15), channel_id=1, source_target_pairs={{0,2},{1,3},{2,0},{3,1},{4,6},{5,7},{6,4},{7,5},{8,10},{9,11},{10,... | collective-permute-start | bytes 98312 | tf_op jit(solution)/shard_map/ppermute | solution.py:67
  57.0 2.1 %collective-permute-done.1 = bf16[32,512]{1,0:T(8,128)(2,1)S(1)} collective-permute-done((bf16[32,512]{1,0:T(8,128)(2,1)S(1)}, bf16[32,512]{1,0:T(8,128)(2,1)S(1)}, u32[]{:S(2)}, u32[]{:S(2)}) %collective-permute-start.1) | collective-permute-done | bytes 32800 | tf_op jit(solution)/shard_map/ppermute | solution.py:67
  60.1 12.7 %all_to_all.29 = bf16[8,32,512]{2,1,0:T(8,128)(2,1)S(1)} all-to-all(bf16[8,32,512]{2,1,0:T(8,128)(2,1)S(1)} %all_to_all.22), channel_id=1, replica_groups=mesh['ep'=8,'tp'=4] {'ep'}, dimensions={0} | all-to-all | bytes 524288 | tf_op jit(solution)/shard_map/all_to_all | solution.py:213
  73.7 5.7 %collective-permute-done.3 = bf16[1,256,512]{2,1,0:T(8,128)(2,1)S(1)} collective-permute-done((bf16[1,256,512]{2,1,0:T(8,128)(2,1)S(1)}, bf16[1,256,512]{2,1,0:T(8,128)(2,1)S(1)}, u32[]{:S(2)}, u32[]{:S(2)}) %collective-permute-start.3) | collective-permute-done | bytes 262176 | tf_op jit(solution)/shard_map/ppermute | solution.py:67
  79.6 2.6 %copy.61 = bf16[2048,384]{1,0:T(8,128)(2,1)} copy(bf16[2048,384]{0,1:T(8,128)(2,1)} %bitcast.130) | data formatting | bytes 3145728 | tf_op jit(solution)/shard_map/dot_general | solution.py:225
  82.7 1.3 %fusion.16 = bf16[256,4,512]{2,0,1:T(8,128)(2,1)} fusion(bf16[2,2,256,512]{3,2,1,0:T(8,128)(2,1)S(1)} %pad_maximum_fusion, f32[4,512]{1,0:T(4,128)S(1)} %reshape.187, f32[256]{0:T(256)S(1)} %add_rsqrt_fusion), kind=kLoop, calls=%fused_computation.19 | loop fusion | flops 2097152 | bytes 2106368 | tf_op jit(solution)/shard_map/convert_element_type | solution.py:12
  84.0 1.5 %copy.52 = bf16[256,4,512]{0,2,1:T(8,128)(2,1)S(1)} copy(bf16[256,4,512]{2,0,1:T(8,128)(2,1)} %fusion.16) | data formatting | bytes 2097152 | tf_op jit(solution)/shard_map/convert_element_type | solution.py:12
  85.5 2.1 %fusion.5 = f32[256,384]{1,0:T(8,128)S(1)} fusion(bf16[256,2048]{0,1:T(8,128)(2,1)S(1)} %bitcast.128, bf16[1,2048,384]{2,1,0:T(8,128)(2,1)} %param.37), kind=kOutput, calls=%fused_computation.8 | convolution fusion | flops 402653184 | bytes 3014656 | tf_op jit(solution)/shard_map/dot_general | solution.py:222
  87.6 4.1 %fusion.21 = f32[256,2,2,512]{3,0,2,1:T(8,128)} fusion(bf16[2,2,512,384]{3,2,1,0:T(8,128)(2,1)} %bitcast.131, bf16[256,2048]{0,1:T(8,128)(2,1)S(1)} %bitcast.129, bf16[1,2048,384]{2,1,0:T(8,128)(2,1)S(1)} %copy-done, f32[256,384]{1,0:T(8,128)S(1)} %fusion.5), kind=kOutput, calls=%fused_computation.27 | convolution fusion | flops 805896192 | bytes 6684672 | tf_op jit(solution)/shard_map/dot_general | solution.py:225
  91.8 1.6 %fusion.23 = bf16[256,2,512]{2,0,1:T(8,128)(2,1)S(1)} fusion(f32[256,2,2,512]{3,0,2,1:T(8,128)} %fusion.21, pred[]{:T(512)S(6)} %eq.29), kind=kLoop, calls=%fused_computation.28 | loop fusion | flops 262144 | bytes 1572865 | tf_op jit(solution)/shard_map/convert_element_type | solution.py:97
  93.9 1.5 %collective-permute-done.5 = bf16[256,2,512]{2,0,1:T(8,128)(2,1)S(1)} collective-permute-done((bf16[256,2,512]{2,0,1:T(8,128)(2,1)S(1)}, bf16[256,2,512]{2,0,1:T(8,128)(2,1)S(1)}, u32[]{:S(2)}, u32[]{:S(2)}) %collective-permute-start.5) | collective-permute-done | bytes 524320 | tf_op jit(solution)/shard_map/ppermute | solution.py:67
  95.5 1.8 %fusion.19 = f32[256,1,2,512]{3,0,2,1:T(8,128)S(1)} fusion(bf16[256,2,512]{2,0,1:T(8,128)(2,1)S(1)} %collective-permute-done.5, f32[256,2,2,512]{3,0,2,1:T(8,128)} %fusion.21, pred[]{:T(512)S(6)} %eq.29), kind=kLoop, calls=%fused_computation.24 | loop fusion | flops 786432 | bytes 3670017 | tf_op jit(solution)/shard_map/reshape | solution.py:94
  98.4 7.7 %collective-permute-done.6 = bf16[256,1,512]{2,0,1:T(8,128)(2,1)S(1)} collective-permute-done((bf16[256,1,512]{2,0,1:T(8,128)(2,1)S(1)}, bf16[256,1,512]{2,0,1:T(8,128)(2,1)S(1)}, u32[]{:S(2)}, u32[]{:S(2)}) %collective-permute-start.6) | collective-permute-done | bytes 262176 | tf_op jit(solution)/shard_map/ppermute | solution.py:67
  106.9 4.7 %all-to-all-start.3 = ((bf16[8,32,512]{2,1,0:T(8,128)(2,1)}), bf16[8,32,512]{2,1,0:T(8,128)(2,1)S(1)}, u32[]{:S(2)}, u32[]{:S(2)}) async-start(bf16[8,32,512]{2,1,0:T(8,128)(2,1)} %bitcast.38), calls=%async_computation.3 | async-start | bytes 524288 | tf_op jit(solution)/shard_map/all_to_all | solution.py:227
  111.7 8.5 %all-to-all-done.3 = bf16[8,32,512]{2,1,0:T(8,128)(2,1)S(1)} async-done(((bf16[8,32,512]{2,1,0:T(8,128)(2,1)}), bf16[8,32,512]{2,1,0:T(8,128)(2,1)S(1)}, u32[]{:S(2)}, u32[]{:S(2)}) %all-to-all-start.3) | async-done | bytes 262176 | tf_op jit(solution)/shard_map/all_to_all | solution.py:227
  (86 shorter events, 11.4 us)
Async XLA Ops:
  0.6 87.0 %copy-start = (bf16[1,2048,384]{2,1,0:T(8,128)(2,1)S(1)}, bf16[1,2048,384]{2,1,0:T(8,128)(2,1)}, u32[]{:S(2)}) copy-start(bf16[1,2048,384]{2,1,0:T(8,128)(2,1)} %param.38) | copy-start | bytes 4718596
  0.6 29.0 %copy-start.4 = (bf16[256,256]{1,0:T(8,128)(2,1)S(1)}, bf16[256,256]{1,0:T(8,128)(2,1)}, u32[]{:S(2)}) copy-start(bf16[256,256]{1,0:T(8,128)(2,1)} %param.23) | copy-start | bytes 393220
  11.4 14.7 %all-to-all-start = ((bf16[8,32,256]{2,1,0:T(8,128)(2,1)}), bf16[8,32,256]{2,1,0:T(8,128)(2,1)S(1)}, u32[]{:S(2)}, u32[]{:S(2)}) async-start(bf16[8,32,256]{2,1,0:T(8,128)(2,1)} %constant_dynamic-update-slice_fusion), calls=%async_computation | async-start | bytes 262144 | tf_op jit(solution)/shard_map/all_to_all | solution.py:153
  27.2 7.3 %copy-start.6 = (bf16[2048]{0:T(1024)(128)(2,1)S(1)}, bf16[2048]{0:T(1024)(128)(2,1)}, u32[]{:S(2)}) copy-start(bf16[2048]{0:T(1024)(128)(2,1)} %param.21) | copy-start | bytes 12292
  27.2 7.3 %copy-start.3 = (bf16[32,2048]{1,0:T(8,128)(2,1)S(1)}, bf16[32,2048]{1,0:T(8,128)(2,1)}, u32[]{:S(2)}) copy-start(bf16[32,2048]{1,0:T(8,128)(2,1)} %param.20) | copy-start | bytes 393220
  27.3 7.3 %copy-start.12 = (bf16[2048,8]{0,1:T(8,128)(2,1)S(1)}, bf16[2048,8]{0,1:T(8,128)(2,1)}, u32[]{:S(2)}) copy-start(bf16[2048,8]{0,1:T(8,128)(2,1)} %param.27) | copy-start | bytes 98308
  27.3 7.3 %copy-start.14 = (f32[8]{0:T(128)S(1)}, f32[8]{0:T(128)}, u32[]{:S(2)}) copy-start(f32[8]{0:T(128)} %param.29) | copy-start | bytes 100
  28.5 6.3 %copy-start.13 = (bf16[2048,8]{0,1:T(8,128)(2,1)S(1)}, bf16[2048,8]{0,1:T(8,128)(2,1)}, u32[]{:S(2)}) copy-start(bf16[2048,8]{0,1:T(8,128)(2,1)} %param.28) | copy-start | bytes 98308
  28.5 6.3 %copy-start.15 = (f32[8]{0:T(128)S(1)}, f32[8]{0:T(128)}, u32[]{:S(2)}) copy-start(f32[8]{0:T(128)} %param.30) | copy-start | bytes 100
  29.7 5.3 %copy-start.10 = (f32[32,2]{0,1:T(2,128)S(1)}, f32[32,2]{0,1:T(2,128)}, u32[]{:S(2)}) copy-start(f32[32,2]{0,1:T(2,128)} %param.34) | copy-start | bytes 772
  30.0 18.1 %copy-start.5 = (f32[32,2,128]{2,1,0:T(2,128)S(1)}, f32[32,2,128]{2,1,0:T(2,128)}, u32[]{:S(2)}) copy-start(f32[32,2,128]{2,1,0:T(2,128)} %param.33) | copy-start | bytes 98308
  31.0 16.8 %all-to-all-start.1 = ((bf16[8,32,1024]{2,1,0:T(8,128)(2,1)}), bf16[8,32,1024]{2,1,0:T(8,128)(2,1)S(1)}, u32[]{:S(2)}, u32[]{:S(2)}) async-start(bf16[8,32,1024]{2,1,0:T(8,128)(2,1)} %bitcast.9), calls=%async_computation.1 | async-start | bytes 1048576 | tf_op jit(solution)/shard_map/all_to_all | solution.py:165
  35.0 17.5 %copy-start.9 = (f32[32,2]{0,1:T(2,128)}, f32[32,2]{0,1:T(2,128)S(1)}, u32[]{:S(2)}) copy-start(f32[32,2]{0,1:T(2,128)S(1)} %get-tuple-element.8) | copy-start | bytes 772
  52.5 2.0 %copy-start.1 = (f32[32,2,128,128]{3,2,1,0:T(8,128)}, f32[32,2,128,128]{3,2,1,0:T(8,128)S(1)}, u32[]{:S(2)}) copy-start(f32[32,2,128,128]{3,2,1,0:T(8,128)S(1)} %multiply_add_fusion) | copy-start | bytes 12582916
  52.5 2.2 %copy-start.2 = (bf16[256,2048]{1,0:T(8,128)(2,1)S(1)}, bf16[256,2048]{1,0:T(8,128)(2,1)}, u32[]{:S(2)}) copy-start(bf16[256,2048]{1,0:T(8,128)(2,1)} %param.31) | copy-start | bytes 3145732
  54.7 24.9 %copy-start.7 = (bf16[2048]{0:T(1024)(128)(2,1)S(1)}, bf16[2048]{0:T(1024)(128)(2,1)}, u32[]{:S(2)}) copy-start(bf16[2048]{0:T(1024)(128)(2,1)} %param.22) | copy-start | bytes 12292
  55.0 1.9 %collective-permute-start = (bf16[32,512]{1,0:T(8,128)(2,1)S(1)}, bf16[32,512]{1,0:T(8,128)(2,1)S(1)}, u32[]{:S(2)}, u32[]{:S(2)}) collective-permute-start(bf16[32,512]{1,0:T(8,128)(2,1)S(1)} %get-tuple-element.13), channel_id=1, source_target_pairs={{0,1},{1,0},{2,3},{3,2},{4,5},{5,4},{6,7},{7,6},{8,9},{9,8},{10,11... | collective-permute-start | bytes 98312 | tf_op jit(solution)/shard_map/ppermute | solution.py:67
  55.1 4.0 %collective-permute-start.1 = (bf16[32,512]{1,0:T(8,128)(2,1)S(1)}, bf16[32,512]{1,0:T(8,128)(2,1)S(1)}, u32[]{:S(2)}, u32[]{:S(2)}) collective-permute-start(bf16[32,512]{1,0:T(8,128)(2,1)S(1)} %get-tuple-element.15), channel_id=1, source_target_pairs={{0,2},{1,3},{2,0},{3,1},{4,6},{5,7},{6,4},{7,5},{8,10},{9,11},{10,... | collective-permute-start | bytes 98312 | tf_op jit(solution)/shard_map/ppermute | solution.py:67
  56.7 3.4 %collective-permute-start.2 = (bf16[32,512]{1,0:T(8,128)(2,1)S(1)}, bf16[32,512]{1,0:T(8,128)(2,1)S(1)}, u32[]{:S(2)}, u32[]{:S(2)}) collective-permute-start(bf16[32,512]{1,0:T(8,128)(2,1)S(1)} %get-tuple-element.14), channel_id=1, source_target_pairs={{0,3},{1,2},{2,1},{3,0},{4,7},{5,6},{6,5},{7,4},{8,11},{9,10},{10,... | collective-permute-start | bytes 98312 | tf_op jit(solution)/shard_map/ppermute | solution.py:67
  72.8 6.6 %collective-permute-start.3 = (bf16[1,256,512]{2,1,0:T(8,128)(2,1)S(1)}, bf16[1,256,512]{2,1,0:T(8,128)(2,1)S(1)}, u32[]{:S(2)}, u32[]{:S(2)}) collective-permute-start(bf16[1,256,512]{2,1,0:T(8,128)(2,1)S(1)} %bitcast.132), channel_id=1, source_target_pairs={{0,2},{1,3},{2,0},{3,1},{4,6},{5,7},{6,4},{7,5},{8,10},{9,11},{10,... | collective-permute-start | bytes 786440 | tf_op jit(solution)/shard_map/ppermute | solution.py:67
  79.5 2.7 %collective-permute-start.4 = (bf16[2,256,512]{2,1,0:T(8,128)(2,1)S(1)}, bf16[2,256,512]{2,1,0:T(8,128)(2,1)S(1)}, u32[]{:S(2)}, u32[]{:S(2)}) collective-permute-start(bf16[2,256,512]{2,1,0:T(8,128)(2,1)S(1)} %maximum_bitcast_fusion), channel_id=1, source_target_pairs={{0,1},{1,0},{2,3},{3,2},{4,5},{5,4},{6,7},{7,6},{8,9},{9,8},{10,11... | collective-permute-start | bytes 1572872 | tf_op jit(solution)/shard_map/ppermute | solution.py:67
  93.4 2.1 %collective-permute-start.5 = (bf16[256,2,512]{2,0,1:T(8,128)(2,1)S(1)}, bf16[256,2,512]{2,0,1:T(8,128)(2,1)S(1)}, u32[]{:S(2)}, u32[]{:S(2)}) collective-permute-start(bf16[256,2,512]{2,0,1:T(8,128)(2,1)S(1)} %fusion.23), channel_id=1, source_target_pairs={{0,1},{1,0},{2,3},{3,2},{4,5},{5,4},{6,7},{7,6},{8,9},{9,8},{10,11... | collective-permute-start | bytes 1572872 | tf_op jit(solution)/shard_map/ppermute | solution.py:67
  97.3 14.3 %copy-start.8 = (f32[32,2]{0,1:T(2,128)S(1)}, f32[32,2]{0,1:T(2,128)}, u32[]{:S(2)}) copy-start(f32[32,2]{0,1:T(2,128)} %param.36) | copy-start | bytes 772
  97.3 14.3 %copy-start.11 = (s32[32,2]{0,1:T(2,128)S(1)}, s32[32,2]{0,1:T(2,128)}, u32[]{:S(2)}) copy-start(s32[32,2]{0,1:T(2,128)} %param.35) | copy-start | bytes 772
  97.4 8.7 %collective-permute-start.6 = (bf16[256,1,512]{2,0,1:T(8,128)(2,1)S(1)}, bf16[256,1,512]{2,0,1:T(8,128)(2,1)S(1)}, u32[]{:S(2)}, u32[]{:S(2)}) collective-permute-start(bf16[256,1,512]{2,0,1:T(8,128)(2,1)S(1)} %fusion.33), channel_id=1, source_target_pairs={{0,2},{1,3},{2,0},{3,1},{4,6},{5,7},{6,4},{7,5},{8,10},{9,11},{10,... | collective-permute-start | bytes 786440 | tf_op jit(solution)/shard_map/ppermute | solution.py:67
  106.9 13.3 %all-to-all-start.3 = ((bf16[8,32,512]{2,1,0:T(8,128)(2,1)}), bf16[8,32,512]{2,1,0:T(8,128)(2,1)S(1)}, u32[]{:S(2)}, u32[]{:S(2)}) async-start(bf16[8,32,512]{2,1,0:T(8,128)(2,1)} %bitcast.38), calls=%async_computation.3 | async-start | bytes 524288 | tf_op jit(solution)/shard_map/all_to_all | solution.py:227
